TPU v7x, 256 devices: a 4x2x16 block of a 4x16x16 slice. The times are simulated.
256 devices in a mesh: grp: 2 (over y), ep: 32 (over z, core), tp: 4 (over x).
Axes of the slice: x: 4, y: 2, z: 16, core: 2. Of those that a mesh axis runs over, the one named last changes fastest.
The devices are a block of a 4x16x16 slice.
Arguments:
- queries: bfloat16 [24576, 1024], P(('grp', 'ep'), 'tp'), parts along dimension 0, may hold values from -6 to 6
- key_values: bfloat16 [24576, 512], P(('grp', 'ep'), 'tp'), parts along dimension 0, may hold values from -6 to 6
- query_gain: float32 [64], replicated, may hold values from 0.5 to 5
- key_gain: float32 [64], replicated, may hold values from 0.5 to 5
- out_weight: bfloat16 [1024, 2048], P('tp'), may hold values from -0.1875 to 0.1875
- second_batch: bfloat16 [32768, 2048], P(('grp', 'ep', 'tp')), parts along dimension 0, may hold values from -6 to 6
- norm_gain: float32 [2048], replicated, may hold values from 0.1 to 1.9
- routes: int32 [32768, 2], P(('grp', 'ep', 'tp')), parts along dimension 0, may hold values from 0 to 63, all different within a row; in each aligned block of 128 rows (0 to 127, 128 to 255, ...) at most 6 rows name the same one
- route_weights: float32 [32768, 2], P(('grp', 'ep', 'tp')), parts along dimension 0, may hold values from 0.2 to 1
- expert_gate: bfloat16 [64, 2048, 1024], P('ep', None, 'tp'), may hold values from -0.125 to 0.125
- expert_up: bfloat16 [64, 2048, 1024], P('ep', None, 'tp'), may hold values from -0.125 to 0.125
- expert_down: bfloat16 [64, 1024, 2048], P('ep', 'tp'), may hold values from -0.1875 to 0.1875
- shared_gate: bfloat16 [2048, 512], P(None, 'tp'), may hold values from -0.125 to 0.125
- shared_up: bfloat16 [2048, 512], P(None, 'tp'), may hold values from -0.125 to 0.125
- shared_down: bfloat16 [512, 2048], P('tp'), may hold values from -0.25 to 0.25
Outputs:
- mixer_out: bfloat16 [24576, 2048], P(('grp', 'ep', 'tp')), parts along dimension 0
- channel_out: bfloat16 [32768, 2048], P(('grp', 'ep', 'tp')), parts along dimension 0
There are 2 independent parts, one for each index of `grp`. A program takes and returns all parts, laid end to end along the dimension named above; an argument that names none is the same for every part. Nothing has to cross between parts.
Inputs may be any that keep to these rules, and one draw needn't show every extreme that they name: `routes`: each row names 2 different experts. Among the rows of one device no expert is named more than 6 times, and in every draw some expert is named exactly 6 times by the rows of some device.
All inputs are finite; a program needn't handle non-finite values.
Results may differ from a plain program's by a relative error of at most 0.015.
The roundings to bfloat16 on the way count: a program that leaves them out, or rounds other values in their place, can miss the bound.
Values may be sent and summed in bfloat16 or wider, within the bound.
A program may use at most 128 MiB of HBM per device.

v0:
```python
import jax
import jax.numpy as jnp
from jax import lax
from jax.sharding import Mesh
from jax.sharding import PartitionSpec as P

GRID_W = 64
EP = ("ep_0", "ep_1")
GRP_EP = ("grp", "ep_0", "ep_1")
GRP_EP_TP = ("grp", "ep_0", "ep_1", "tp")
rope_base = 10000.0
norm_eps = 1e-06


def joined_along(tiles, dim):
    shape = list(tiles.shape[1:])
    shape[dim] *= tiles.shape[0]
    return jnp.moveaxis(tiles, 0, dim).reshape(shape)


def stacked_from(shard, axes, order):
    tiles = shard
    for k in order:
        tiles = lax.all_gather(tiles, axes[k])
    done = order[::-1]
    back = [done.index(k) for k in range(len(axes))]
    tiles = tiles.transpose(*back, *range(len(axes), tiles.ndim))
    return tiles.reshape(-1, *shard.shape)


def whole_of(shard, axes, order, dim):
    return joined_along(stacked_from(shard, axes, order), dim)


def from_everyone(shard, axis):
    copies = jnp.broadcast_to(shard, (lax.axis_size(axis), *shard.shape))
    return lax.all_to_all(copies, axis, split_axis=0, concat_axis=0, tiled=True)


def gathered_copies(shard, axis, dim):
    return joined_along(from_everyone(shard, axis), dim)


def in_blocks(shard, dim, length):
    shape = shard.shape
    tiles = shard.reshape(*shape[:dim], length, shape[dim] // length, *shape[dim + 1 :])
    return jnp.moveaxis(tiles, dim, 0)


def summed_on_arrival(shard, axis, dim):
    tiles = in_blocks(shard, dim, lax.axis_size(axis))
    arrived = lax.all_to_all(tiles, axis, split_axis=0, concat_axis=0, tiled=True)
    return arrived.astype(jnp.float32).sum(axis=0)


def head_norm(vectors, gain):
    return (
        vectors * lax.rsqrt(jnp.mean(vectors * vectors, axis=-1, keepdims=True) + norm_eps) * gain
    )


def turn_heads(vectors, positions):
    row_count, head_count, head_size = vectors.shape
    half_size = head_size // 2
    inverse = rope_base ** (-jnp.arange(0, half_size, 2, dtype=jnp.float32) / half_size)
    grid_row = (positions // GRID_W).astype(jnp.float32)
    grid_column = (positions % GRID_W).astype(jnp.float32)
    angles = jnp.concatenate([grid_row[:, None] * inverse, grid_column[:, None] * inverse], axis=-1)
    cosine = jnp.cos(angles)[:, None, :]
    sine = jnp.sin(angles)[:, None, :]
    paired = vectors.reshape(row_count, head_count, half_size, 2)
    first = paired[..., 0]
    second = paired[..., 1]
    turned = jnp.stack([first * cosine - second * sine, first * sine + second * cosine], axis=-1)
    return turned.reshape(vectors.shape)


def slot_ids(route_rows, expert_count, capacity):
    row_count, top_count = route_rows.shape
    flat_routes = route_rows.reshape(-1)
    onehot = (flat_routes[:, None] == jnp.arange(expert_count, dtype=jnp.int32)[None, :]).astype(
        jnp.int32
    )
    earlier = jnp.cumsum(onehot, axis=0) - onehot
    within = jnp.sum(earlier * onehot, axis=1)
    return (flat_routes * capacity + within).reshape(row_count, top_count)


def slot_table(slots, slot_count):
    row_count, top_count = slots.shape
    flat_slots = slots.reshape(-1)
    owner_row = jnp.arange(row_count * top_count, dtype=jnp.int32) // top_count
    matches = flat_slots[None, :] == jnp.arange(slot_count, dtype=jnp.int32)[:, None]
    occupied = jnp.any(matches, axis=1)
    source_row = jnp.sum(jnp.where(matches, owner_row[None, :], 0), axis=1)
    return jnp.where(occupied, source_row, row_count)


def pick_block(row_count):
    for candidate in range(min(row_count, 1024), 0, -1):
        if row_count % candidate == 0:
            return candidate
    return row_count


def attend_keys(query_turned, scale, running, pieces):
    head_size = query_turned.shape[-1]
    key_block = pick_block(pieces.shape[0])
    blocks = pieces.reshape(pieces.shape[0] // key_block, key_block, 2 * head_size)

    def one_block(carried, block_rows):
        top_now, total_now, acc_now = carried
        scores = (
            jnp.einsum(
                "qhd,kd->hqk",
                query_turned,
                block_rows[:, :head_size],
                preferred_element_type=jnp.float32,
            )
            * scale
        )
        top_new = jnp.maximum(top_now, jnp.max(scores, axis=-1))
        shrink = jnp.exp(top_now - top_new)
        exps = jnp.exp(scores - top_new[..., None])
        total_new = total_now * shrink + jnp.sum(exps, axis=-1)
        acc_new = acc_now * shrink[..., None] + jnp.einsum(
            "hqk,kd->hqd",
            exps.astype(jnp.bfloat16),
            block_rows[:, head_size:],
            preferred_element_type=jnp.float32,
        )
        return ((top_new, total_new, acc_new), None)

    result, ignored = lax.scan(one_block, running, blocks)
    return result


def shared_hidden_of(token_rows, gate_weights, up_weights):
    gate_part = jnp.dot(token_rows, gate_weights, preferred_element_type=jnp.float32)
    up_part = jnp.dot(token_rows, up_weights, preferred_element_type=jnp.float32)
    return (jax.nn.silu(gate_part) * up_part).astype(jnp.bfloat16)


def expert_hidden(slot_rows, gate_weights, up_weights):
    gate_part = jnp.einsum(
        "osjcd,jdf->osjcf", slot_rows, gate_weights, preferred_element_type=jnp.float32
    )
    up_part = jnp.einsum(
        "osjcd,jdf->osjcf", slot_rows, up_weights, preferred_element_type=jnp.float32
    )
    return (jax.nn.silu(gate_part) * up_part).astype(jnp.bfloat16)


def body(
    queries,
    key_values,
    query_gain,
    key_gain,
    out_weight,
    second_batch,
    norm_gain,
    routes,
    route_weights,
    expert_gate,
    expert_up,
    expert_down,
    shared_gate,
    shared_up,
    shared_down,
):
    query_rows = queries.shape[0]
    head_size = query_gain.shape[0]
    heads_here = queries.shape[1] // head_size
    ep_count = lax.axis_size(EP)
    positions = lax.axis_index(EP) * query_rows + jnp.arange(query_rows, dtype=jnp.int32)
    query_turned = turn_heads(
        head_norm(
            queries.reshape(query_rows, heads_here, head_size).astype(jnp.float32), query_gain
        ),
        positions,
    ).astype(jnp.bfloat16)
    key_turned = turn_heads(
        head_norm(key_values[:, None, :head_size].astype(jnp.float32), key_gain), positions
    ).astype(jnp.bfloat16)
    keys_and_values = jnp.concatenate([key_turned[:, 0, :], key_values[:, head_size:]], axis=1)
    start_state = (
        jnp.full((heads_here, query_rows), -1e30, jnp.float32),
        jnp.zeros((heads_here, query_rows), jnp.float32),
        jnp.zeros((heads_here, query_rows, head_size), jnp.float32),
    )
    top_all, total_all, acc_all = attend_keys(
        query_turned, head_size ** (-0.5), start_state, whole_of(keys_and_values, EP, (0, 1), 0)
    )
    head_out = (
        (acc_all / total_all[..., None])
        .transpose(1, 0, 2)
        .reshape(query_rows, heads_here * head_size)
        .astype(jnp.bfloat16)
    )
    tok_count = second_batch.shape[0]
    model_width = second_batch.shape[1]
    top_count = routes.shape[1]
    local_experts = expert_gate.shape[0]
    expert_count = local_experts * ep_count
    capacity = 3 * tok_count * top_count // (2 * expert_count)
    slot_count = expert_count * capacity
    token_float = second_batch.astype(jnp.float32)
    normed = (
        token_float
        * lax.rsqrt(jnp.mean(token_float * token_float, axis=-1, keepdims=True) + norm_eps)
        * norm_gain
    ).astype(jnp.bfloat16)
    own_slots = slot_ids(routes, expert_count, capacity)
    shared_hidden = (lambda pieces, begin_at: shared_hidden_of(pieces, shared_gate, shared_up))(
        gathered_copies(normed, "tp", 0), jnp.int32(0)
    )
    outgoing = jnp.take(
        normed, slot_table(own_slots, slot_count), axis=0, mode="fill", fill_value=0
    )[None]
    arrived = lax.all_to_all(outgoing, EP, split_axis=1, concat_axis=1, tiled=True)
    arrived = arrived.reshape(arrived.shape[0], ep_count, local_experts, capacity, model_width)
    hidden = expert_hidden(
        lax.all_gather(arrived, "tp", axis=0, tiled=True), expert_gate, expert_up
    )
    routed_part = jnp.einsum(
        "osjcf,jfd->osjcd", hidden, expert_down, preferred_element_type=jnp.float32
    ).reshape(-1, model_width)
    shared_part = jnp.dot(shared_hidden, shared_down, preferred_element_type=jnp.float32)
    head_partial = jnp.dot(head_out, out_weight, preferred_element_type=jnp.float32)
    attn_sum, routed_sum, shared_sum = (
        summed_on_arrival(head_partial.astype(jnp.bfloat16), "tp", 0),
        summed_on_arrival(routed_part.astype(jnp.bfloat16), "tp", 0),
        summed_on_arrival(shared_part.astype(jnp.bfloat16), "tp", 0),
    )
    returned = lax.all_to_all(
        routed_sum.astype(jnp.bfloat16), EP, split_axis=0, concat_axis=0, tiled=True
    )
    combined = shared_sum
    for slot_pick in range(top_count):
        combined = combined + route_weights[:, slot_pick : slot_pick + 1] * jnp.take(
            returned, own_slots[:, slot_pick], axis=0
        ).astype(jnp.float32)
    return (attn_sum.astype(jnp.bfloat16), combined.astype(jnp.bfloat16))


def solution(mesh):
    torus = Mesh(
        mesh.devices.reshape(mesh.shape["grp"], 16, 2, mesh.shape["tp"]),
        ("grp", "ep_0", "ep_1", "tp"),
    )
    return jax.shard_map(
        body,
        mesh=torus,
        in_specs=(
            P(GRP_EP, "tp"),
            P(GRP_EP, "tp"),
            P(),
            P(),
            P("tp", None),
            P(GRP_EP_TP, None),
            P(),
            P(GRP_EP_TP, None),
            P(GRP_EP_TP, None),
            P(EP, None, "tp"),
            P(EP, None, "tp"),
            P(EP, "tp", None),
            P(None, "tp"),
            P(None, "tp"),
            P("tp", None),
        ),
        out_specs=(P(GRP_EP_TP, None), P(GRP_EP_TP, None)),
        check_vma=False,
    )
```

profile of v0, /device:TPU:33, one launch (start us, length us, event | category | flops | bytes accessed | tf_op | source)
XLA Modules:
  0.0 621.9 jit_solution(13244901644372939689)
XLA Ops:
  17.1 4.1 copy.120
  21.7 12.4 %reduce.10 = bf16[384,2048]{1,0:T(8,128)(2,1)} reduce(bf16[384,1,2048]{2,1,0:T(2,128)(2,1)} %bitcast.152, bf16[]{:T(256)} %broadcast.416), dimensions={1}, to_apply=%bitcast.134.reduce_sub_computation | reduce | bytes 3145730
  34.1 5.2 reshape.492
  39.3 25.6 %all-to-all-start.3 = ((bf16[32,2,12288]{2,1,0:T(2,128)(2,1)}), bf16[32,2,12288]{2,1,0:T(2,128)(2,1)}, u32[]{:S(2)}, u32[]{:S(2)}) async-start(bf16[32,2,12288]{2,1,0:T(2,128)(2,1)} %reshape.492), calls=%async_computation.3 | async-start | bytes 3145728 | tf_op jit(solution)/shard_map/all_to_all | solution.py:220
  66.8 95.3 %all-gather.8.cloned.1.call-done = bf16[6144,128]{0,1:T(8,128)(2,1)} async-done(((bf16[384,128]{0,1:T(8,128)(2,1)}), bf16[6144,128]{0,1:T(8,128)(2,1)}) %all-gather.8.cloned.1.call-update) | async-done | bytes 1572880 | tf_op jit(solution)/shard_map/all_gather | solution.py:24
  164.9 9.5 %reshape.493 = bf16[384,1,2048]{2,1,0:T(2,128)(2,1)} reshape(bf16[32,2,12288]{2,1,0:T(2,128)(2,1)} %all-to-all-done.3) | data formatting | bytes 3145728
  174.3 12.2 %bitcast_reduce_fusion.2 = bf16[384,2048]{1,0:T(8,128)(2,1)} fusion(bf16[384,1,2048]{2,1,0:T(2,128)(2,1)} %reshape.493), kind=kLoop, calls=%fused_computation.129 | loop fusion | bytes 3145728 | tf_op jit(solution)/shard_map/all_to_all | solution.py:220
  186.6 3.7 reshape.450
  190.3 3.6 copy.99
  195.7 4.8 all-to-all-start.1
  202.6 25.4 %all-to-all-done.1 = bf16[4,128,2048]{2,1,0:T(8,128)(2,1)} async-done(((bf16[4,128,2048]{2,1,0:T(8,128)(2,1)}), bf16[4,128,2048]{2,1,0:T(8,128)(2,1)}, u32[]{:S(2)}, u32[]{:S(2)}) %all-to-all-start.1) | async-done | bytes 2097184 | tf_op jit(solution)/shard_map/all_to_all | solution.py:37
  230.3 5.5 convolution_convert_fusion
  235.8 4.5 all-to-all-start.2
  240.4 4.0 copy.91
  244.4 55.9 %all-gather.6.cloned.1.call-done = bf16[4,32,2,6,2048]{4,1,3,0,2:T(8,128)(2,1)} async-done(((bf16[1,32,2,6,2048]{4,1,3,0,2:T(8,128)(2,1)}), bf16[4,32,2,6,2048]{4,1,3,0,2:T(8,128)(2,1)}) %all-gather.6.cloned.1.call-update) | async-done | bytes 6291472 | tf_op jit(solution)/shard_map/all_gather | solution.py:223
  300.3 6.4 %fusion.14 = f32[2,4,32,6,256]{4,2,3,1,0:T(8,128)} fusion(bf16[4,32,2,6,2048]{4,1,3,0,2:T(8,128)(2,1)} %all-gather.6.cloned.1.call-done, bf16[2,2048,256]{2,1,0:T(8,128)(2,1)} %param.28), kind=kOutput, calls=%fused_computation.27 | convolution fusion | flops 1610612736 | bytes 9961472 | tf_op jit(solution)/shard_map/osjcd,jdf->osjcf/dot_general | solution.py:145
  306.7 10.1 %convert_bitcast_fusion = bf16[4,32,2,6,2048]{4,1,3,0,2:T(8,128)(2,1)} fusion(bf16[2,256,2048]{2,1,0:T(8,128)(2,1)S(1)} %copy-done, f32[2,4,32,6,256]{4,2,3,1,0:T(8,128)} %fusion.14, bf16[4,32,2,6,2048]{4,1,3,0,2:T(8,128)(2,1)} %all-gather.6.cloned.1.call-done, bf16[2,2048,256]{2,1,0:T(8,128)(2,1)} %param.29), kind=kOutput, calls=%fused_computation.20 | convolution fusion | flops 3226730496 | bytes 18350080 | tf_op jit(solution)/shard_map/osjcf,jfd->osjcd/dot_general | solution.py:225
  316.8 10.2 %copy.100 = bf16[4,32,2,6,2048]{4,0,3,2,1:T(4,128)(2,1)} copy(bf16[4,32,2,6,2048]{4,1,3,0,2:T(8,128)(2,1)} %convert_bitcast_fusion) | data formatting | bytes 12582912 | tf_op jit(solution)/shard_map/convert_element_type | solution.py:232
  327.0 9.1 %copy.101 = bf16[4,384,2048]{2,1,0:T(8,128)(2,1)} copy(bf16[4,384,2048]{2,0,1:T(4,128)(2,1)} %bitcast.151) | data formatting | bytes 12582912 | tf_op jit(solution)/shard_map/convert_element_type | solution.py:232
  336.1 5.3 all-to-all-start.4
  341.5 127.8 %while.15 = (s32[]{:T(128)}, f32[4,384]{1,0:T(4,128)S(1)}, f32[4,384]{1,0:T(4,128)S(1)}, f32[4,384,64]{1,2,0:T(8,128)S(1)}, bf16[12,1024,128]{2,1,0:T(8,128)(2,1...) while((s32[]{:T(128)}, f32[4,384]{1,0:T(4,128)S(1)}, f32[4,384]{1,0:T(4,128)S(1)}, ...), condition=%wide.region_5.6_spmd.clone, body=%wide.region_2.5_spmd.clone.sunk | while | flops 415538688 | bytes 46432384 | solution.py:134
  346.3 4.0 fusion.76
  357.0 4.0 fusion.76
  364.0 3.6 bitcast_reduce_fusion.4
  367.6 4.0 fusion.76
  378.2 4.0 fusion.76
  385.3 3.6 bitcast_reduce_fusion.4
  388.9 4.0 fusion.76
  395.9 3.6 bitcast_reduce_fusion.4
  399.5 4.0 fusion.76
  406.5 3.6 bitcast_reduce_fusion.4
  410.2 4.0 fusion.76
  417.2 3.6 bitcast_reduce_fusion.4
  420.8 4.0 fusion.76
  427.8 3.6 bitcast_reduce_fusion.4
  431.5 4.0 fusion.76
  438.5 3.6 bitcast_reduce_fusion.4
  442.1 4.0 fusion.76
  449.1 3.6 bitcast_reduce_fusion.4
  452.8 4.0 fusion.76
  459.8 3.6 bitcast_reduce_fusion.4
  463.4 4.0 fusion.76
  471.1 4.1 all-to-all-start
  475.3 5.7 reduce_sum.96
  484.5 10.4 %all-to-all-done = bf16[4,96,2048]{2,1,0:T(8,128)(2,1)S(1)} async-done(((bf16[4,96,2048]{2,1,0:T(8,128)(2,1)}), bf16[4,96,2048]{2,1,0:T(8,128)(2,1)S(1)}, u32[]{:S(2)}, u32[]{:S(2)}) %all-to-all-start) | async-done | bytes 1572896 | tf_op jit(solution)/shard_map/all_to_all | solution.py:52
  495.0 11.2 %all-to-all-start.5 = ((bf16[32,12,2048]{2,1,0:T(8,128)(2,1)}), bf16[32,12,2048]{2,1,0:T(8,128)(2,1)}, u32[]{:S(2)}, u32[]{:S(2)}) async-start(bf16[32,12,2048]{2,1,0:T(8,128)(2,1)} %all_to_all.28), calls=%async_computation.5 | async-start | bytes 4194304 | tf_op jit(solution)/shard_map/all_to_all | solution.py:235
  509.6 94.8 %all-to-all-done.5 = bf16[32,12,2048]{2,1,0:T(8,128)(2,1)} async-done(((bf16[32,12,2048]{2,1,0:T(8,128)(2,1)}), bf16[32,12,2048]{2,1,0:T(8,128)(2,1)}, u32[]{:S(2)}, u32[]{:S(2)}) %all-to-all-start.5) | async-done | bytes 1572896 | tf_op jit(solution)/shard_map/all_to_all | solution.py:235
  608.7 4.0 gather_fusion.2
  (196 shorter events, 83.5 us)
Async XLA Ops:
  7.2 299.5 %copy-start = (bf16[2,256,2048]{2,1,0:T(8,128)(2,1)S(1)}, bf16[2,256,2048]{2,1,0:T(8,128)(2,1)}, u32[]{:S(2)}) copy-start(bf16[2,256,2048]{2,1,0:T(8,128)(2,1)} %param.30) | copy-start | bytes 6291460
  39.3 25.7 %copy-start.5 = (bf16[384,128]{1,0:T(8,128)(2,1)S(1)}, bf16[384,128]{1,0:T(8,128)(2,1)}, u32[]{:S(2)}) copy-start(bf16[384,128]{1,0:T(8,128)(2,1)} %param.20) | copy-start | bytes 294916
  39.3 26.0 %copy-start.9 = (f32[64]{0:T(128)S(1)}, f32[64]{0:T(128)}, u32[]{:S(2)}) copy-start(f32[64]{0:T(128)} %param.22) | copy-start | bytes 772
  39.3 125.6 %all-to-all-start.3 = ((bf16[32,2,12288]{2,1,0:T(2,128)(2,1)}), bf16[32,2,12288]{2,1,0:T(2,128)(2,1)}, u32[]{:S(2)}, u32[]{:S(2)}) async-start(bf16[32,2,12288]{2,1,0:T(2,128)(2,1)} %reshape.492), calls=%async_computation.3 | async-start | bytes 3145728 | tf_op jit(solution)/shard_map/all_to_all | solution.py:220
  64.9 97.2 %all-gather.8.cloned.1.call-start = ((), (), s32[]{:S(2)}) async-start(), calls=%async_computation.7 | async-start | bytes 1671168 | tf_op jit(solution)/shard_map/all_gather | solution.py:24
  66.7 173.7 %all-gather.10.cloned.1.call-start = ((), (), s32[]{:S(2)}) async-start(), calls=%async_computation.8 | async-start | bytes 4718592 | tf_op jit(solution)/shard_map/all_gather | solution.py:24
  164.8 135.5 %all-gather.6.cloned.1.call-start = ((), (), s32[]{:S(2)}) async-start(), calls=%async_computation.6 | async-start | bytes 7864320 | tf_op jit(solution)/shard_map/all_gather | solution.py:223
  195.7 4.9 copy-start.6
  195.7 5.3 copy-start.10
  195.7 32.2 %all-to-all-start.1 = ((bf16[4,128,2048]{2,1,0:T(8,128)(2,1)}), bf16[4,128,2048]{2,1,0:T(8,128)(2,1)}, u32[]{:S(2)}, u32[]{:S(2)}) async-start(bf16[4,128,2048]{2,1,0:T(8,128)(2,1)} %broadcast_in_dim.47), calls=%async_computation.1 | async-start | bytes 4194304 | tf_op jit(solution)/shard_map/all_to_all | solution.py:37
  235.8 100.3 %all-to-all-start.2 = ((bf16[4,128,2048]{2,1,0:T(8,128)(2,1)}), bf16[4,128,2048]{2,1,0:T(8,128)(2,1)}, u32[]{:S(2)}, u32[]{:S(2)}) async-start(bf16[4,128,2048]{2,1,0:T(8,128)(2,1)} %bitcast.153), calls=%async_computation.2 | async-start | bytes 4194304 | tf_op jit(solution)/shard_map/all_to_all | solution.py:52
  336.1 135.0 %all-to-all-start.4 = ((bf16[4,384,2048]{2,1,0:T(8,128)(2,1)}), bf16[4,384,2048]{2,1,0:T(8,128)(2,1)}, u32[]{:S(2)}, u32[]{:S(2)}) async-start(bf16[4,384,2048]{2,1,0:T(8,128)(2,1)} %copy.101), calls=%async_computation.4 | async-start | bytes 12582912 | tf_op jit(solution)/shard_map/all_to_all | solution.py:52
  341.4 127.9 %copy-start.4 = (bf16[256,2048]{1,0:T(8,128)(2,1)S(1)}, bf16[256,2048]{1,0:T(8,128)(2,1)}, u32[]{:S(2)}) copy-start(bf16[256,2048]{1,0:T(8,128)(2,1)} %param.23) | copy-start | bytes 3145732
  346.3 4.6 copy-start.2
  357.0 4.6 copy-start.2
  367.6 4.6 copy-start.2
  378.2 4.6 copy-start.2
  388.9 4.6 copy-start.2
  399.5 4.6 copy-start.2
  410.2 4.6 copy-start.2
  420.8 4.6 copy-start.2
  431.5 4.6 copy-start.2
  442.1 4.6 copy-start.2
  452.7 4.6 copy-start.2
  463.4 4.6 copy-start.2
  471.1 23.9 %all-to-all-start = ((bf16[4,96,2048]{2,1,0:T(8,128)(2,1)}), bf16[4,96,2048]{2,1,0:T(8,128)(2,1)S(1)}, u32[]{:S(2)}, u32[]{:S(2)}) async-start(bf16[4,96,2048]{2,1,0:T(8,128)(2,1)} %bitcast.156), calls=%async_computation | async-start | bytes 3145728 | tf_op jit(solution)/shard_map/all_to_all | solution.py:52
  484.5 21.8 %copy-start.7 = (s32[128,2]{0,1:T(2,128)S(1)}, s32[128,2]{0,1:T(2,128)}, u32[]{:S(2)}) copy-start(s32[128,2]{0,1:T(2,128)} %param.26) | copy-start | bytes 3076
  484.5 21.9 %copy-start.8 = (f32[128,2]{0,1:T(2,128)S(1)}, f32[128,2]{0,1:T(2,128)}, u32[]{:S(2)}) copy-start(f32[128,2]{0,1:T(2,128)} %param.27) | copy-start | bytes 3076
  495.0 109.4 %all-to-all-start.5 = ((bf16[32,12,2048]{2,1,0:T(8,128)(2,1)}), bf16[32,12,2048]{2,1,0:T(8,128)(2,1)}, u32[]{:S(2)}, u32[]{:S(2)}) async-start(bf16[32,12,2048]{2,1,0:T(8,128)(2,1)} %all_to_all.28), calls=%async_computation.5 | async-start | bytes 4194304 | tf_op jit(solution)/shard_map/all_to_all | solution.py:235
  606.9 1.8 copy-start.3
  608.7 6.4 %copy-start.1 = (bf16[2,256,2048]{2,1,0:T(8,128)(2,1)S(1)}, bf16[2,256,2048]{2,1,0:T(8,128)(2,1)}, u32[]{:S(2)}) copy-start(bf16[2,256,2048]{2,1,0:T(8,128)(2,1)} %param.30) | copy-start | bytes 6291460
Sparse Core Ops, SparseCore 0:
  68.1 93.9 all-gather.7
  164.9 24.2 all-gather.9
  194.1 106.1 all-gather.5
where the time goes:
time: 626 us; the launch traced here: 622 us
  waiting for transfers between devices  282 us (45%)
  local copies, waits for them, and re-layouts  105 us (17%)
  matrix products  84.7 us (14%)
  other arithmetic  79.3 us (13%)
  starting transfers between devices  55.8 us (9%)
  between operations  14.5 us (2%)
    all_gather x2, waiting for transfers between devices, stacked_from(): tiles = lax.all_gather(tiles, axes[k])  95.4 us
    all_to_all x1, waiting for transfers between devices, body(): lax.all_to_all(routed_sum.astype(jnp.bfloat16), EP, split_axis=0, concat_...  94.8 us
    all_gather x1, waiting for transfers between devices, body(): lax.all_gather(arrived, 'tp', axis=0, tiled=True)  55.9 us
    reduce_sum x12, other arithmetic, one_block(): total_new = total_now * shrink + jnp.sum(exps, axis=-1)  47.6 us
    dot_general x12, matrix products, one_block(): jnp.einsum('qhd,kd->hqk', query_turned, block_rows[:, :head_size], prefer...  43.5 us
    all_to_all x1, starting transfers between devices, body(): lax.all_to_all(outgoing, EP, split_axis=1, concat_axis=1, tiled=True)  25.6 us
    all_to_all x1, waiting for transfers between devices, from_everyone(): return lax.all_to_all(copies, axis, split_axis=0, concat_axis=0, tiled=True)  25.4 us
    convert_element_type x2, local copies, waits for them, and re-layouts, body(): routed_part.astype(jnp.bfloat16)  19.3 us
  transfers between devices with their start and end apart: 9, of which 5 were waited for; matrix products, arithmetic and copies ran while one was open for 35% of the time, Pallas kernels for 0%

commit v1 on v0

--- a/solution.py
+++ b/solution.py
@@ -1,3 +1,4 @@
+import functools
 import jax
 import jax.numpy as jnp
 from jax import lax
@@ -10,6 +11,15 @@
 GRP_EP_TP = ("grp", "ep_0", "ep_1", "tp")
 rope_base = 10000.0
 norm_eps = 1e-06
+
+
+def sizes_use(local_x, axis_name):
+    spare = jnp.concatenate([local_x for _ in range(lax.psum(1, axis_name=axis_name))], 0)
+    high = lax.all_to_all(spare, axis_name=axis_name, tiled=True, concat_axis=0, split_axis=0)
+    return high
+
+
+launch_wires_on_mesh = functools.partial(sizes_use, axis_name="tp")
 
 
 def joined_along(tiles, dim):
@@ -219,9 +229,7 @@
     )[None]
     arrived = lax.all_to_all(outgoing, EP, split_axis=1, concat_axis=1, tiled=True)
     arrived = arrived.reshape(arrived.shape[0], ep_count, local_experts, capacity, model_width)
-    hidden = expert_hidden(
-        lax.all_gather(arrived, "tp", axis=0, tiled=True), expert_gate, expert_up
-    )
+    hidden = expert_hidden(launch_wires_on_mesh(arrived), expert_gate, expert_up)
     routed_part = jnp.einsum(
         "osjcf,jfd->osjcd", hidden, expert_down, preferred_element_type=jnp.float32
     ).reshape(-1, model_width)

time: 626 us -> 589 us (0.941)
  waiting for transfers between devices: 282 us -> 238 us
    all_to_all x1, waiting for transfers between devices: 0.01 us -> 77 us  [body(): lax.all_to_all(outgoing, EP, split_axis=1, concat_axis=1, tiled=True)]
    all_gather x2, waiting for transfers between devices: 95.4 us -> 35 us  [stacked_from(): tiles = lax.all_gather(tiles, axes[k])]
    all_gather x1 -> x0, waiting for transfers between devices: 55.9 us -> none  [body(): lax.all_gather(arrived, 'tp', axis=0, tiled=True)]
    all_to_all x1, waiting for transfers between devices: 25.4 us -> 0.01 us  [from_everyone(): return lax.all_to_all(copies, axis, split_axis=0, concat_axis=0, tiled=True)]
    all_to_all x0 -> x1, waiting for transfers between devices: none -> 19.2 us  [sizes_use(): lax.all_to_all(spare, axis_name=axis_name, tiled=True, concat_axis=0, spl...]
  transfers between devices with their start and end apart: 9 -> 9, of which waited for: 5 -> 6; matrix products, arithmetic and copies ran while one was open for 35% -> 37% of each run, Pallas kernels for 0% -> 0%
where the time goes in v1:
time: 589 us; the launch traced here: 584 us
  waiting for transfers between devices  238 us (40%)
  local copies, waits for them, and re-layouts  110 us (19%)
  matrix products  84.7 us (14%)
  other arithmetic  79.3 us (13%)
  starting transfers between devices  57.1 us (10%)
  between operations  14.7 us (2%)
    all_to_all x1, waiting for transfers between devices, body(): lax.all_to_all(routed_sum.astype(jnp.bfloat16), EP, split_axis=0, concat_...  96.8 us
    all_to_all x1, waiting for transfers between devices, body(): lax.all_to_all(outgoing, EP, split_axis=1, concat_axis=1, tiled=True)  77 us
    reduce_sum x12, other arithmetic, one_block(): total_new = total_now * shrink + jnp.sum(exps, axis=-1)  47.6 us
    dot_general x12, matrix products, one_block(): jnp.einsum('qhd,kd->hqk', query_turned, block_rows[:, :head_size], prefer...  43.5 us
    all_gather x2, waiting for transfers between devices, stacked_from(): tiles = lax.all_gather(tiles, axes[k])  35 us
    all_to_all x1, starting transfers between devices, body(): lax.all_to_all(outgoing, EP, split_axis=1, concat_axis=1, tiled=True)  25.6 us
    convert_element_type x2, local copies, waits for them, and re-layouts, body(): routed_part.astype(jnp.bfloat16)  19.3 us
    all_to_all x1, waiting for transfers between devices, sizes_use(): lax.all_to_all(spare, axis_name=axis_name, tiled=True, concat_axis=0, spl...  19.2 us
  transfers between devices with their start and end apart: 9, of which 6 were waited for; matrix products, arithmetic and copies ran while one was open for 37% of the time, Pallas kernels for 0%

profile of v1, /device:TPU:33, one launch (start us, length us, event | category | flops | bytes accessed | tf_op | source)
XLA Modules:
  0.0 584.1 jit_solution(6906188248415132187)
XLA Ops:
  17.1 4.1 copy.135
  21.7 12.4 %reduce.10 = bf16[384,2048]{1,0:T(8,128)(2,1)} reduce(bf16[384,1,2048]{2,1,0:T(2,128)(2,1)} %bitcast.150, bf16[]{:T(256)} %broadcast.417), dimensions={1}, to_apply=%bitcast.132.reduce_sub_computation | reduce | bytes 3145730
  34.1 5.0 reshape.494
  39.1 25.6 %all-to-all-start.3 = ((bf16[32,2,12288]{2,1,0:T(2,128)(2,1)}), bf16[32,2,12288]{2,1,0:T(2,128)(2,1)}, u32[]{:S(2)}, u32[]{:S(2)}) async-start(bf16[32,2,12288]{2,1,0:T(2,128)(2,1)} %reshape.494), calls=%async_computation.3 | async-start | bytes 3145728 | tf_op jit(solution)/shard_map/all_to_all | solution.py:230
  65.5 77.0 %all-to-all-done.3 = bf16[32,2,12288]{2,1,0:T(2,128)(2,1)} async-done(((bf16[32,2,12288]{2,1,0:T(2,128)(2,1)}), bf16[32,2,12288]{2,1,0:T(2,128)(2,1)}, u32[]{:S(2)}, u32[]{:S(2)}) %all-to-all-start.3) | async-done | bytes 1572896 | tf_op jit(solution)/shard_map/all_to_all | solution.py:230
  144.2 4.5 all-to-all-start.1
  149.7 9.5 %reshape.495 = bf16[384,1,2048]{2,1,0:T(2,128)(2,1)} reshape(bf16[32,2,12288]{2,1,0:T(2,128)(2,1)} %all-to-all-done.3) | data formatting | bytes 3145728
  159.2 12.2 %bitcast_reduce_fusion.2 = bf16[384,2048]{1,0:T(8,128)(2,1)} fusion(bf16[384,1,2048]{2,1,0:T(2,128)(2,1)} %reshape.495), kind=kLoop, calls=%fused_computation.131 | loop fusion | bytes 3145728 | tf_op jit(solution)/shard_map/all_to_all | solution.py:230
  171.5 4.1 reshape.452
  179.2 4.9 concatenate.45
  184.1 5.3 all-to-all-start.4
  189.5 16.3 %all-gather.5.cloned.1.call-done = bf16[6144,128]{0,1:T(8,128)(2,1)} async-done(((bf16[384,128]{0,1:T(8,128)(2,1)}), bf16[6144,128]{0,1:T(8,128)(2,1)}) %all-gather.5.cloned.1.call-update) | async-done | bytes 1572880 | tf_op jit(solution)/shard_map/all_gather | solution.py:34
  212.9 5.5 convolution_convert_fusion
  218.4 18.7 %all-gather.7.cloned.1.call-done = bf16[32,384,128]{2,1,0:T(8,128)(2,1)} async-done(((bf16[16,384,128]{2,1,0:T(8,128)(2,1)}), bf16[32,384,128]{2,1,0:T(8,128)(2,1)}) %all-gather.7.cloned.1.call-update) | async-done | bytes 3145744 | tf_op jit(solution)/shard_map/all_gather | solution.py:34
  237.1 3.9 copy.96
  241.0 19.2 %all-to-all-done.4 = bf16[4,32,2,6,2048]{4,1,3,2,0:T(8,128)(2,1)} async-done(((bf16[4,32,2,6,2048]{4,1,3,2,0:T(8,128)(2,1)}), bf16[4,32,2,6,2048]{4,1,3,2,0:T(8,128)(2,1)}, u32[]{:S(2)}, u32[]{:S(2)}) %all-to-all-start.4) | async-done | bytes 6291488 | tf_op jit(solution)/shard_map/all_to_all | solution.py:18
  260.2 4.7 all-to-all-start.2
  265.0 6.4 %fusion.13 = f32[2,4,32,6,256]{4,2,3,1,0:T(8,128)} fusion(bf16[4,32,2,6,2048]{4,1,3,2,0:T(8,128)(2,1)} %all-to-all-done.4, bf16[2,2048,256]{2,1,0:T(8,128)(2,1)} %param.28), kind=kOutput, calls=%fused_computation.23 | convolution fusion | flops 1610612736 | bytes 9961472 | tf_op jit(solution)/shard_map/osjcd,jdf->osjcf/dot_general | solution.py:155
  271.4 10.1 %convert_bitcast_fusion = bf16[4,32,2,6,2048]{4,1,3,0,2:T(8,128)(2,1)} fusion(bf16[2,256,2048]{2,1,0:T(8,128)(2,1)S(1)} %copy-done, f32[2,4,32,6,256]{4,2,3,1,0:T(8,128)} %fusion.13, bf16[2,2048,256]{2,1,0:T(8,128)(2,1)} %param.29, bf16[4,32,2,6,2048]{4,1,3,2,0:T(8,128)(2,1)} %all-to-all-done.4), kind=kOutput, calls=%fused_computation.20 | convolution fusion | flops 3226730496 | bytes 18350080 | tf_op jit(solution)/shard_map/osjcf,jfd->osjcd/dot_general | solution.py:233
  281.4 10.2 %copy.107 = bf16[4,32,2,6,2048]{4,0,3,2,1:T(4,128)(2,1)} copy(bf16[4,32,2,6,2048]{4,1,3,0,2:T(8,128)(2,1)} %convert_bitcast_fusion) | data formatting | bytes 12582912 | tf_op jit(solution)/shard_map/convert_element_type | solution.py:240
  291.7 9.1 %copy.108 = bf16[4,384,2048]{2,1,0:T(8,128)(2,1)} copy(bf16[4,384,2048]{2,0,1:T(4,128)(2,1)} %bitcast.149) | data formatting | bytes 12582912 | tf_op jit(solution)/shard_map/convert_element_type | solution.py:240
  300.8 5.3 all-to-all-start.5
  306.1 127.8 %while.15 = (s32[]{:T(128)}, f32[4,384]{1,0:T(4,128)S(1)}, f32[4,384]{1,0:T(4,128)S(1)}, f32[4,384,64]{1,2,0:T(8,128)S(1)}, bf16[12,1024,128]{2,1,0:T(8,128)(2,1...) while((s32[]{:T(128)}, f32[4,384]{1,0:T(4,128)S(1)}, f32[4,384]{1,0:T(4,128)S(1)}, ...), condition=%wide.region_5.6_spmd.clone, body=%wide.region_2.5_spmd.clone.sunk | while | flops 415538688 | bytes 46432384 | solution.py:144
  307.4 3.6 bitcast_reduce_fusion.4
  311.0 4.0 fusion.80
  318.0 3.6 bitcast_reduce_fusion.4
  321.6 4.0 fusion.80
  328.6 3.6 bitcast_reduce_fusion.4
  332.3 4.0 fusion.80
  339.3 3.6 bitcast_reduce_fusion.4
  342.9 4.0 fusion.80
  349.9 3.6 bitcast_reduce_fusion.4
  353.6 4.0 fusion.80
  364.2 4.0 fusion.80
  371.2 3.6 bitcast_reduce_fusion.4
  374.9 4.0 fusion.80
  381.9 3.6 bitcast_reduce_fusion.4
  385.5 4.0 fusion.80
  396.1 4.0 fusion.80
  406.8 4.0 fusion.80
  417.4 4.0 fusion.80
  428.1 4.0 fusion.80
  435.8 4.1 all-to-all-start
  439.9 5.7 reduce_sum.96
  449.2 9.6 %all-to-all-done = bf16[4,96,2048]{2,1,0:T(8,128)(2,1)S(1)} async-done(((bf16[4,96,2048]{2,1,0:T(8,128)(2,1)}), bf16[4,96,2048]{2,1,0:T(8,128)(2,1)S(1)}, u32[]{:S(2)}, u32[]{:S(2)}) %all-to-all-start) | async-done | bytes 1572896 | tf_op jit(solution)/shard_map/all_to_all | solution.py:62
  458.8 7.3 %all-to-all-start.6 = ((bf16[32,12,2048]{2,1,0:T(8,128)(2,1)}), bf16[32,12,2048]{2,1,0:T(8,128)(2,1)}, u32[]{:S(2)}, u32[]{:S(2)}) async-start(bf16[32,12,2048]{2,1,0:T(8,128)(2,1)} %all_to_all.32), calls=%async_computation.6 | async-start | bytes 4194304 | tf_op jit(solution)/shard_map/all_to_all | solution.py:243
  469.6 96.8 %all-to-all-done.6 = bf16[32,12,2048]{2,1,0:T(8,128)(2,1)} async-done(((bf16[32,12,2048]{2,1,0:T(8,128)(2,1)}), bf16[32,12,2048]{2,1,0:T(8,128)(2,1)}, u32[]{:S(2)}, u32[]{:S(2)}) %all-to-all-start.6) | async-done | bytes 1572896 | tf_op jit(solution)/shard_map/all_to_all | solution.py:243
  570.6 4.0 gather_fusion.2
  (196 shorter events, 94.1 us)
Async XLA Ops:
  7.2 264.2 %copy-start = (bf16[2,256,2048]{2,1,0:T(8,128)(2,1)S(1)}, bf16[2,256,2048]{2,1,0:T(8,128)(2,1)}, u32[]{:S(2)}) copy-start(bf16[2,256,2048]{2,1,0:T(8,128)(2,1)} %param.30) | copy-start | bytes 6291460
  39.1 25.6 %copy-start.5 = (bf16[384,128]{1,0:T(8,128)(2,1)S(1)}, bf16[384,128]{1,0:T(8,128)(2,1)}, u32[]{:S(2)}) copy-start(bf16[384,128]{1,0:T(8,128)(2,1)} %param.20) | copy-start | bytes 294916
  39.1 25.9 %copy-start.9 = (f32[64]{0:T(128)S(1)}, f32[64]{0:T(128)}, u32[]{:S(2)}) copy-start(f32[64]{0:T(128)} %param.22) | copy-start | bytes 772
  39.1 103.5 %all-to-all-start.3 = ((bf16[32,2,12288]{2,1,0:T(2,128)(2,1)}), bf16[32,2,12288]{2,1,0:T(2,128)(2,1)}, u32[]{:S(2)}, u32[]{:S(2)}) async-start(bf16[32,2,12288]{2,1,0:T(2,128)(2,1)} %reshape.494), calls=%async_computation.3 | async-start | bytes 3145728 | tf_op jit(solution)/shard_map/all_to_all | solution.py:230
  144.2 34.9 %all-to-all-start.1 = ((bf16[4,128,2048]{2,1,0:T(8,128)(2,1)}), bf16[4,128,2048]{2,1,0:T(8,128)(2,1)}, u32[]{:S(2)}, u32[]{:S(2)}) async-start(bf16[4,128,2048]{2,1,0:T(8,128)(2,1)} %broadcast_in_dim.47), calls=%async_computation.1 | async-start | bytes 4194304 | tf_op jit(solution)/shard_map/all_to_all | solution.py:47
  148.8 57.0 %all-gather.5.cloned.1.call-start = ((), (), s32[]{:S(2)}) async-start(), calls=%async_computation.7 | async-start | bytes 1671168 | tf_op jit(solution)/shard_map/all_gather | solution.py:34
  184.1 76.2 %all-to-all-start.4 = ((bf16[4,32,2,6,2048]{4,1,3,2,0:T(8,128)(2,1)}), bf16[4,32,2,6,2048]{4,1,3,2,0:T(8,128)(2,1)}, u32[]{:S(2)}, u32[]{:S(2)}) async-start(bf16[4,32,2,6,2048]{4,1,3,2,0:T(8,128)(2,1)} %concatenate.45), calls=%async_computation.4 | async-start | bytes 12582912 | tf_op jit(solution)/shard_map/all_to_all | solution.py:18
  189.4 19.1 %copy-start.6 = (bf16[384,256]{1,0:T(8,128)(2,1)S(1)}, bf16[384,256]{1,0:T(8,128)(2,1)}, u32[]{:S(2)}) copy-start(bf16[384,256]{1,0:T(8,128)(2,1)} %param.19) | copy-start | bytes 589828
  189.4 19.5 %copy-start.10 = (f32[64]{0:T(128)S(1)}, f32[64]{0:T(128)}, u32[]{:S(2)}) copy-start(f32[64]{0:T(128)} %param.21) | copy-start | bytes 772
  189.4 47.7 %all-gather.7.cloned.1.call-start = ((), (), s32[]{:S(2)}) async-start(), calls=%async_computation.8 | async-start | bytes 4718592 | tf_op jit(solution)/shard_map/all_gather | solution.py:34
  260.2 40.6 %all-to-all-start.2 = ((bf16[4,128,2048]{2,1,0:T(8,128)(2,1)}), bf16[4,128,2048]{2,1,0:T(8,128)(2,1)}, u32[]{:S(2)}, u32[]{:S(2)}) async-start(bf16[4,128,2048]{2,1,0:T(8,128)(2,1)} %bitcast.151), calls=%async_computation.2 | async-start | bytes 4194304 | tf_op jit(solution)/shard_map/all_to_all | solution.py:62
  300.8 135.0 %all-to-all-start.5 = ((bf16[4,384,2048]{2,1,0:T(8,128)(2,1)}), bf16[4,384,2048]{2,1,0:T(8,128)(2,1)}, u32[]{:S(2)}, u32[]{:S(2)}) async-start(bf16[4,384,2048]{2,1,0:T(8,128)(2,1)} %copy.108), calls=%async_computation.5 | async-start | bytes 12582912 | tf_op jit(solution)/shard_map/all_to_all | solution.py:62
  306.1 127.9 %copy-start.4 = (bf16[256,2048]{1,0:T(8,128)(2,1)S(1)}, bf16[256,2048]{1,0:T(8,128)(2,1)}, u32[]{:S(2)}) copy-start(bf16[256,2048]{1,0:T(8,128)(2,1)} %param.23) | copy-start | bytes 3145732
  311.0 4.6 copy-start.2
  321.6 4.6 copy-start.2
  332.3 4.6 copy-start.2
  342.9 4.6 copy-start.2
  353.6 4.6 copy-start.2
  364.2 4.6 copy-start.2
  374.9 4.6 copy-start.2
  385.5 4.6 copy-start.2
  396.1 4.6 copy-start.2
  406.8 4.6 copy-start.2
  417.4 4.6 copy-start.2
  428.1 4.6 copy-start.2
  435.8 23.0 %all-to-all-start = ((bf16[4,96,2048]{2,1,0:T(8,128)(2,1)}), bf16[4,96,2048]{2,1,0:T(8,128)(2,1)S(1)}, u32[]{:S(2)}, u32[]{:S(2)}) async-start(bf16[4,96,2048]{2,1,0:T(8,128)(2,1)} %bitcast.154), calls=%async_computation | async-start | bytes 3145728 | tf_op jit(solution)/shard_map/all_to_all | solution.py:62
  449.2 17.1 %copy-start.7 = (s32[128,2]{0,1:T(2,128)S(1)}, s32[128,2]{0,1:T(2,128)}, u32[]{:S(2)}) copy-start(s32[128,2]{0,1:T(2,128)} %param.26) | copy-start | bytes 3076
  449.2 17.2 %copy-start.8 = (f32[128,2]{0,1:T(2,128)S(1)}, f32[128,2]{0,1:T(2,128)}, u32[]{:S(2)}) copy-start(f32[128,2]{0,1:T(2,128)} %param.27) | copy-start | bytes 3076
  458.8 107.6 %all-to-all-start.6 = ((bf16[32,12,2048]{2,1,0:T(8,128)(2,1)}), bf16[32,12,2048]{2,1,0:T(8,128)(2,1)}, u32[]{:S(2)}, u32[]{:S(2)}) async-start(bf16[32,12,2048]{2,1,0:T(8,128)(2,1)} %all_to_all.32), calls=%async_computation.6 | async-start | bytes 4194304 | tf_op jit(solution)/shard_map/all_to_all | solution.py:243
  568.9 1.8 copy-start.3
  570.6 6.4 %copy-start.1 = (bf16[2,256,2048]{2,1,0:T(8,128)(2,1)S(1)}, bf16[2,256,2048]{2,1,0:T(8,128)(2,1)}, u32[]{:S(2)}) copy-start(bf16[2,256,2048]{2,1,0:T(8,128)(2,1)} %param.30) | copy-start | bytes 6291460
Sparse Core Ops, SparseCore 0:
  152.0 53.7 all-gather.4
  208.6 28.4 all-gather.6
